TPU v7x, 256 devices: a whole 4x4x8 slice. The times are simulated.
256 devices in a mesh: sp: 16 (over y, x), dp: 16 (over z, core).
Axes of the slice: x: 4, y: 4, z: 8, core: 2. Of those that a mesh axis runs over, the one named last changes fastest.
Arguments:
- tokens: bfloat16 [16, 2048, 2048], P('dp', 'sp'), may hold values from -6 to 6
- query_weight: bfloat16 [2048, 1024], P('dp'), may hold values from -0.125 to 0.125
- key_weight: bfloat16 [2048, 1024], P('dp'), may hold values from -0.125 to 0.125
- value_weight: bfloat16 [2048, 2048], P('dp'), may hold values from -0.125 to 0.125
- output_weight: bfloat16 [2048, 2048], P('dp'), may hold values from -0.125 to 0.125
- log_decay: float32 [2, 16], P(None, 'sp'), may hold values from -0.04 to 0, as said below
Outputs:
- mixed: bfloat16 [16, 2048, 2048], P('dp', 'sp')
Inputs may be any that keep to these rules, and one draw needn't show every extreme that they name: `log_decay`: every entry is negative: the logarithm of a head's decay per position.
All inputs are finite; a program needn't handle non-finite values.
Results may differ from a plain program's by a relative error of at most 0.012.
Values may be sent and summed in bfloat16 or wider, within the bound.
No kernel may reach another device: no remote copies, remote signals or barrier semaphores. Data moves between devices by JAX's collectives and lax.ppermute only.
A program may use at most 128 MiB of HBM per device.

v0:
```python
import jax
import jax.numpy as jnp
from jax import lax
from jax.sharding import PartitionSpec as P

HEADS = 16
DK = 64
DV = 128
BLOCK = 512


def in_order(pieces, dim):
    lengths = list(pieces.shape[1:])
    lengths[dim] *= pieces.shape[0]
    return jnp.moveaxis(pieces, 0, dim).reshape(lengths)


def copy_for_each(shard, axis):
    count = lax.axis_size(axis)
    return lax.all_to_all(
        jnp.broadcast_to(shard[None], (count, *shard.shape)), axis, 0, 0, tiled=True
    )


def gathered_copies(shard, axis, dim):
    return in_order(copy_for_each(shard, axis), dim)


def rotate(values_part, positions):
    half_dim = values_part.shape[-1] // 2
    frequency = 10000.0 ** (-jnp.arange(half_dim, dtype=jnp.float32) / half_dim)
    angles = positions[:, None] * frequency[None, :]
    cosine = jnp.cos(angles)[:, None, :]
    sine_part = jnp.sin(angles)[:, None, :]
    first = values_part[..., :half_dim]
    second = values_part[..., half_dim:]
    return jnp.concatenate(
        [first * cosine - second * sine_part, first * sine_part + second * cosine], axis=-1
    )


def retain(query, key_rows, value_rows, log_rate):
    length, heads, key_dim = query.shape
    value_dim = value_rows.shape[-1]
    count = length // BLOCK
    offsets = jnp.arange(BLOCK, dtype=jnp.float32)
    distance = offsets[:, None] - offsets[None, :]
    decay_inner = jnp.where(
        distance[None] >= 0.0,
        jnp.exp(log_rate[:, None, None] * jnp.maximum(distance, 0.0)[None]),
        0.0,
    )
    decay_query = jnp.exp((offsets[:, None] + 1.0) * log_rate[None, :])[:, :, None]
    decay_key = jnp.exp((BLOCK - 1.0 - offsets)[:, None] * log_rate[None, :])[:, :, None]
    decay_block = jnp.exp(BLOCK * log_rate)[:, None, None]

    def blocks(array):
        return array.reshape(count, BLOCK, heads, array.shape[-1])

    def advance(state, inputs):
        query_block, key_block, value_block = inputs
        inner = (
            jnp.einsum("ihd,jhd->hij", query_block, key_block, preferred_element_type=jnp.float32)
            * decay_inner
        )
        result = jnp.einsum(
            "hij,jhv->ihv",
            inner.astype(jnp.bfloat16),
            value_block,
            preferred_element_type=jnp.float32,
        )
        query_wide = query_block.astype(jnp.float32) * decay_query
        result = result + jnp.einsum("ihd,hdv->ihv", query_wide, state)
        key_wide = key_block.astype(jnp.float32) * decay_key
        state = state * decay_block + jnp.einsum(
            "jhd,jhv->hdv", key_wide, value_block.astype(jnp.float32)
        )
        return (state, result)

    initial = jnp.zeros((heads, key_dim, value_dim), jnp.float32)
    final_state, outputs = lax.scan(
        advance, initial, (blocks(query), blocks(key_rows), blocks(value_rows))
    )
    return outputs.reshape(length, heads, value_dim)


def mechanism(stacked, log_decay):
    length = stacked.shape[0]
    widened = stacked[..., : 2 * DK].astype(jnp.float32)
    positions = jnp.arange(length, dtype=jnp.float32)
    query = rotate(widened[..., :DK], positions).astype(jnp.bfloat16)
    key_rows = rotate(widened[..., DK : 2 * DK], positions).astype(jnp.bfloat16)
    value_rows = stacked[..., 2 * DK :]
    forward = retain(query, key_rows, value_rows, log_decay[0])
    backward = retain(
        jnp.flip(query, 0), jnp.flip(key_rows, 0), jnp.flip(value_rows, 0), log_decay[1]
    )
    combined = forward + jnp.flip(backward, 0)
    average = jnp.mean(combined, axis=-1, keepdims=True)
    centred = combined - average
    variance = jnp.mean(centred * centred, axis=-1, keepdims=True)
    return (centred * lax.rsqrt(variance + 1e-06)).astype(jnp.bfloat16)


def shards(tokens, query_weight, key_weight, value_weight, output_weight, log_decay):
    rows = tokens[0]
    row_count = rows.shape[0]
    local_heads = log_decay.shape[1]
    first_head = lax.axis_index("sp") * local_heads
    own_slices = jnp.concatenate(
        [
            lax.dynamic_slice_in_dim(query_weight, first_head * DK, local_heads * DK, 1),
            lax.dynamic_slice_in_dim(key_weight, first_head * DK, local_heads * DK, 1),
            lax.dynamic_slice_in_dim(value_weight, first_head * DV, local_heads * DV, 1),
        ],
        axis=1,
    )
    own_whole = gathered_copies(own_slices, "dp", 0)
    piece = lax.all_gather(rows, "sp", axis=0, tiled=True)
    count = piece.shape[0]
    product = jnp.dot(piece, own_whole, preferred_element_type=jnp.float32).astype(jnp.bfloat16)
    query_part = product[:, : local_heads * DK].reshape(count, local_heads, DK)
    key_part = product[:, local_heads * DK : 2 * local_heads * DK].reshape(count, local_heads, DK)
    value_part = product[:, 2 * local_heads * DK :].reshape(count, local_heads, DV)
    gathered = jnp.concatenate([query_part, key_part, value_part], axis=2)
    normed = mechanism(gathered, log_decay)
    by_token = lax.all_to_all(normed, "sp", split_axis=0, concat_axis=1, tiled=True).reshape(
        row_count, HEADS * DV
    )
    mixed = jnp.dot(
        by_token,
        lax.all_gather(output_weight, "dp", axis=0, tiled=True),
        preferred_element_type=jnp.float32,
    )
    return mixed.astype(jnp.bfloat16)[None]


def solution(mesh):
    placed = (
        P("dp", "sp", None),
        P("dp", None),
        P("dp", None),
        P("dp", None),
        P("dp", None),
        P(None, "sp"),
    )
    return jax.shard_map(
        shards, mesh=mesh, in_specs=placed, out_specs=P("dp", "sp", None), check_vma=False
    )
```

profile of v0, /device:TPU:32, one launch (start us, length us, event | category | flops | bytes accessed | tf_op | source)
XLA Modules:
  0.0 171.1 jit_solution(11749039148471384118)
XLA Ops:
  6.5 0.7 all-gather.6.cloned.1.call-update
  7.3 0.7 all-gather.4.cloned.1.call-update
  8.0 0.9 constant_dynamic-slice_fusion.1
  9.0 1.1 broadcast_in_dim.18
  10.1 8.6 %all-to-all-start = ((bf16[16,128,256]{2,1,0:T(8,128)(2,1)}), bf16[16,128,256]{2,1,0:T(8,128)(2,1)S(1)}, u32[]{:S(2)}, u32[]{:S(2)}) async-start(bf16[16,128,256]{2,1,0:T(8,128)(2,1)} %broadcast_in_dim.18), calls=%async_computation | async-start | bytes 2097152 | tf_op jit(solution)/shard_map/all_to_all | solution.py:20
  18.7 1.4 fusion.116
  21.5 21.8 %all-to-all-done = bf16[16,128,256]{2,1,0:T(8,128)(2,1)S(1)} async-done(((bf16[16,128,256]{2,1,0:T(8,128)(2,1)}), bf16[16,128,256]{2,1,0:T(8,128)(2,1)S(1)}, u32[]{:S(2)}, u32[]{:S(2)}) %all-to-all-start) | async-done | bytes 1048608 | tf_op jit(solution)/shard_map/all_to_all | solution.py:20
  43.3 45.0 %all-gather.6.cloned.1.call-done = bf16[1,2048,2048]{2,1,0:T(8,128)(2,1)} async-done(((bf16[1,128,2048]{2,1,0:T(8,128)(2,1)}), bf16[1,2048,2048]{2,1,0:T(8,128)(2,1)}) %all-gather.6.cloned.1.call-update) | async-done | bytes 8388624 | tf_op jit(solution)/shard_map/all_gather | solution.py:119
  88.3 5.8 %fusion.109 = bf16[2048,256]{0,1:T(8,128)(2,1)S(1)} fusion(bf16[2048,256]{1,0:T(8,128)(2,1)S(1)} %bitcast.255, bf16[1,2048,2048]{2,1,0:T(8,128)(2,1)} %all-gather.6.cloned.1.call-done), kind=kOutput, calls=%fused_computation.103 | convolution fusion | flops 2148007936 | bytes 10485760 | tf_op jit(solution)/shard_map/dot_general | solution.py:121
  94.1 1.0 copy.52
  95.1 1.6 reverse.3
  96.9 1.2 subtract_convert_fusion
  98.3 1.4 rev.14
  99.7 1.4 rev.13
  101.1 0.8 copy.76
  102.2 17.2 %while.31 = (s32[]{:T(128)}, f32[1,64,128]{2,1,0:T(8,128)S(1)}, f32[4,512,1,128]{3,1,0,2:T(8,128)S(1)}, f32[1,1,1]{2,1,0:T(1,128)}, bf16[4,512,1,64]{1,3,2,0:T(8...) while((s32[]{:T(128)}, f32[1,64,128]{2,1,0:T(8,128)S(1)}, ...), condition=%wide.region_3.4_spmd.clone.clone.clone, body=%wide.region_2.3_spmd.clone.clone.clone.sunk | while | flops 119506944 | bytes 2469500 | solution.py:81
  102.2 2.2 %fusion.158 = f32[128,512]{1,0:T(8,128)S(1)} fusion(f32[]{:T(128)} %get-tuple-element.508, bf16[4,512,1,128]{3,1,2,0:T(8,128)(2,1)S(1)} %get-tuple-element.506, s32[]{:T(128)} %get-tuple-element.491, bf16[4,512,1,64]{1,3,2,0:T(8,128)(2,1)S(1)} %get-tuple-element.507, bf16[4,512,1,64]{1,3,2,0:T(8,128)(2,1)} %get-tuple-element.505), kind=kOutput, calls=%fused_computation.55.clone.1 | convolution fusion | flops 102498304 | bytes 526336 | tf_op jit(solution)/shard_map/while/body/eval_jaxpr/hij,jhv->ihv/dot_general | solution.py:66
  104.4 0.7 multiply_exponential_fusion.7
  105.5 1.0 fusion.157
  106.5 2.2 %fusion.158 = f32[128,512]{1,0:T(8,128)S(1)} fusion(f32[]{:T(128)} %get-tuple-element.508, bf16[4,512,1,128]{3,1,2,0:T(8,128)(2,1)S(1)} %get-tuple-element.506, s32[]{:T(128)} %get-tuple-element.491, bf16[4,512,1,64]{1,3,2,0:T(8,128)(2,1)S(1)} %get-tuple-element.507, bf16[4,512,1,64]{1,3,2,0:T(8,128)(2,1)} %get-tuple-element.505), kind=kOutput, calls=%fused_computation.55.clone.1 | convolution fusion | flops 102498304 | bytes 526336 | tf_op jit(solution)/shard_map/while/body/eval_jaxpr/hij,jhv->ihv/dot_general | solution.py:66
  108.7 0.7 multiply_exponential_fusion.7
  109.8 1.0 fusion.157
  110.9 2.2 %fusion.158 = f32[128,512]{1,0:T(8,128)S(1)} fusion(f32[]{:T(128)} %get-tuple-element.508, bf16[4,512,1,128]{3,1,2,0:T(8,128)(2,1)S(1)} %get-tuple-element.506, s32[]{:T(128)} %get-tuple-element.491, bf16[4,512,1,64]{1,3,2,0:T(8,128)(2,1)S(1)} %get-tuple-element.507, bf16[4,512,1,64]{1,3,2,0:T(8,128)(2,1)} %get-tuple-element.505), kind=kOutput, calls=%fused_computation.55.clone.1 | convolution fusion | flops 102498304 | bytes 526336 | tf_op jit(solution)/shard_map/while/body/eval_jaxpr/hij,jhv->ihv/dot_general | solution.py:66
  113.1 0.7 multiply_exponential_fusion.7
  114.1 1.0 fusion.157
  115.2 2.2 %fusion.158 = f32[128,512]{1,0:T(8,128)S(1)} fusion(f32[]{:T(128)} %get-tuple-element.508, bf16[4,512,1,128]{3,1,2,0:T(8,128)(2,1)S(1)} %get-tuple-element.506, s32[]{:T(128)} %get-tuple-element.491, bf16[4,512,1,64]{1,3,2,0:T(8,128)(2,1)S(1)} %get-tuple-element.507, bf16[4,512,1,64]{1,3,2,0:T(8,128)(2,1)} %get-tuple-element.505), kind=kOutput, calls=%fused_computation.55.clone.1 | convolution fusion | flops 102498304 | bytes 526336 | tf_op jit(solution)/shard_map/while/body/eval_jaxpr/hij,jhv->ihv/dot_general | solution.py:66
  117.4 0.7 multiply_exponential_fusion.7
  118.5 1.0 fusion.157
  119.9 0.7 pad_maximum_fusion
  120.7 17.5 %while.30 = (s32[]{:T(128)}, f32[1,64,128]{2,1,0:T(8,128)S(1)}, f32[4,512,1,128]{3,1,0,2:T(8,128)S(1)}, f32[1,1,1]{2,1,0:T(1,128)}, bf16[4,512,1,64]{1,3,2,0:T(8...) while((s32[]{:T(128)}, f32[1,64,128]{2,1,0:T(8,128)S(1)}, ...), condition=%wide.region_1.2_spmd.clone.clone.clone, body=%wide.region_0.1_spmd.clone.clone.clone.sunk | while | flops 119506944 | bytes 2469500 | solution.py:81
  120.7 2.2 %fusion.148 = f32[128,512]{1,0:T(8,128)S(1)} fusion(f32[]{:T(128)} %get-tuple-element.538, bf16[4,512,1,128]{3,1,2,0:T(8,128)(2,1)} %get-tuple-element.536, s32[]{:T(128)} %get-tuple-element.521, bf16[4,512,1,64]{1,3,2,0:T(8,128)(2,1)S(1)} %get-tuple-element.537, bf16[4,512,1,64]{1,3,2,0:T(8,128)(2,1)} %get-tuple-element.535), kind=kOutput, calls=%fused_computation.8.clone.1 | convolution fusion | flops 102498304 | bytes 526336 | tf_op jit(solution)/shard_map/while/body/eval_jaxpr/hij,jhv->ihv/dot_general | solution.py:66
  122.9 0.6 multiply_exponential_fusion.6
  124.0 1.1 fusion.147
  125.1 2.2 %fusion.148 = f32[128,512]{1,0:T(8,128)S(1)} fusion(f32[]{:T(128)} %get-tuple-element.538, bf16[4,512,1,128]{3,1,2,0:T(8,128)(2,1)} %get-tuple-element.536, s32[]{:T(128)} %get-tuple-element.521, bf16[4,512,1,64]{1,3,2,0:T(8,128)(2,1)S(1)} %get-tuple-element.537, bf16[4,512,1,64]{1,3,2,0:T(8,128)(2,1)} %get-tuple-element.535), kind=kOutput, calls=%fused_computation.8.clone.1 | convolution fusion | flops 102498304 | bytes 526336 | tf_op jit(solution)/shard_map/while/body/eval_jaxpr/hij,jhv->ihv/dot_general | solution.py:66
  127.3 0.6 multiply_exponential_fusion.6
  128.3 1.1 fusion.147
  129.4 2.2 %fusion.148 = f32[128,512]{1,0:T(8,128)S(1)} fusion(f32[]{:T(128)} %get-tuple-element.538, bf16[4,512,1,128]{3,1,2,0:T(8,128)(2,1)} %get-tuple-element.536, s32[]{:T(128)} %get-tuple-element.521, bf16[4,512,1,64]{1,3,2,0:T(8,128)(2,1)S(1)} %get-tuple-element.537, bf16[4,512,1,64]{1,3,2,0:T(8,128)(2,1)} %get-tuple-element.535), kind=kOutput, calls=%fused_computation.8.clone.1 | convolution fusion | flops 102498304 | bytes 526336 | tf_op jit(solution)/shard_map/while/body/eval_jaxpr/hij,jhv->ihv/dot_general | solution.py:66
  131.7 0.6 multiply_exponential_fusion.6
  132.7 1.1 fusion.147
  133.8 2.2 %fusion.148 = f32[128,512]{1,0:T(8,128)S(1)} fusion(f32[]{:T(128)} %get-tuple-element.538, bf16[4,512,1,128]{3,1,2,0:T(8,128)(2,1)} %get-tuple-element.536, s32[]{:T(128)} %get-tuple-element.521, bf16[4,512,1,64]{1,3,2,0:T(8,128)(2,1)S(1)} %get-tuple-element.537, bf16[4,512,1,64]{1,3,2,0:T(8,128)(2,1)} %get-tuple-element.535), kind=kOutput, calls=%fused_computation.8.clone.1 | convolution fusion | flops 102498304 | bytes 526336 | tf_op jit(solution)/shard_map/while/body/eval_jaxpr/hij,jhv->ihv/dot_general | solution.py:66
  136.0 0.6 multiply_exponential_fusion.6
  137.1 1.1 fusion.147
  138.5 0.6 multiply_reduce_fusion
  139.2 0.6 multiply_convert_fusion
  140.3 1.0 reduce.2
  141.5 16.4 %all_to_all.20 = bf16[16,2,8192]{2,1,0:T(2,128)(2,1)S(1)} all-to-all(bf16[16,2,8192]{2,1,0:T(2,128)(2,1)S(1)} %reshape.742), channel_id=1, replica_groups=mesh['sp'=16,'dp'=16] {'sp'}, dimensions={0} | all-to-all | bytes 1048576 | tf_op jit(solution)/shard_map/all_to_all | solution.py:127
  157.9 0.5 reshape.743
  158.8 5.5 %fusion.112 = bf16[1,128,2048]{2,1,0:T(8,128)(2,1)} fusion(bf16[128,2048]{0,1:T(8,128)(2,1)S(1)} %bitcast.246, bf16[2048,2048]{1,0:T(8,128)(2,1)} %all-gather.4.cloned.1.call-done), kind=kOutput, calls=%fused_computation.105 | convolution fusion | flops 1074003968 | bytes 9437184 | tf_op jit(solution)/shard_map/dot_general | solution.py:130
  (56 shorter events, 5.6 us)
Async XLA Ops:
  6.5 1.5 copy-start
  6.5 81.7 %all-gather.6.cloned.1.call-start = ((), (), s32[]{:S(2)}) async-start(), calls=%async_computation.3 | async-start | bytes 8912896 | tf_op jit(solution)/shard_map/all_gather | solution.py:119
  7.3 151.5 %all-gather.4.cloned.1.call-start = ((), (), s32[]{:S(2)}) async-start(), calls=%async_computation.2 | async-start | bytes 8912896 | tf_op jit(solution)/shard_map/all_gather | solution.py:132
  10.1 33.2 %all-to-all-start = ((bf16[16,128,256]{2,1,0:T(8,128)(2,1)}), bf16[16,128,256]{2,1,0:T(8,128)(2,1)S(1)}, u32[]{:S(2)}, u32[]{:S(2)}) async-start(bf16[16,128,256]{2,1,0:T(8,128)(2,1)} %broadcast_in_dim.18), calls=%async_computation | async-start | bytes 2097152 | tf_op jit(solution)/shard_map/all_to_all | solution.py:20
Sparse Core Ops, SparseCore 0:
  9.8 78.4 all-gather.5
  90.1 53.8 all-gather.3
where the time goes:
time: 172 us; the launch traced here: 171 us
  waiting for transfers between devices  68.2 us (40%)
  matrix products  39 us (23%)
  blocking collectives  16.4 us (10%)
  between operations  15 us (9%)
  local copies, waits for them, and re-layouts  13.2 us (8%)
  other arithmetic  10.2 us (6%)
  starting transfers between devices  8.63 us (5%)
    all_gather x1, waiting for transfers between devices, shards(): piece = lax.all_gather(rows, 'sp', axis=0, tiled=True)  45 us
    all_to_all x1, waiting for transfers between devices, copy_for_each(): lax.all_to_all(jnp.broadcast_to(shard[None], (count, *shard.shape)), axis...  21.8 us
    dot_general x8, matrix products, advance(): jnp.einsum('hij,jhv->ihv', inner.astype(jnp.bfloat16), value_block, prefe...  17.5 us
    all_to_all x1, blocking collectives, shards(): lax.all_to_all(normed, 'sp', split_axis=0, concat_axis=1, tiled=True)  16.4 us
    all_to_all x1, starting transfers between devices, copy_for_each(): lax.all_to_all(jnp.broadcast_to(shard[None], (count, *shard.shape)), axis...  8.59 us
    dot_general x8, matrix products, advance(): jnp.einsum('jhd,jhv->hdv', key_wide, value_block.astype(jnp.float32))  8.43 us
    dot_general x1, matrix products, shards(): jnp.dot(piece, own_whole, preferred_element_type=jnp.float32)  5.77 us
    dot_general x1, matrix products, shards(): jnp.dot(by_token, lax.all_gather(output_weight, 'dp', axis=0, tiled=True)...  5.47 us
  transfers between devices with their start and end apart: 3, of which 2 were waited for; matrix products, arithmetic and copies ran while one was open for 33% of the time, Pallas kernels for 0%

commit v1 on v0

--- a/solution.py
+++ b/solution.py
@@ -116,7 +116,9 @@
         axis=1,
     )
     own_whole = gathered_copies(own_slices, "dp", 0)
-    piece = lax.all_gather(rows, "sp", axis=0, tiled=True)
+    peers = lax.axis_size("sp")
+    repeats = [peers if d == 0 else 1 for d in range(rows.ndim)]
+    piece = lax.all_to_all(jnp.tile(rows, repeats), "sp", split_axis=0, concat_axis=0, tiled=True)
     count = piece.shape[0]
     product = jnp.dot(piece, own_whole, preferred_element_type=jnp.float32).astype(jnp.bfloat16)
     query_part = product[:, : local_heads * DK].reshape(count, local_heads, DK)

time: 172 us -> 270 us (1.57); the launches traced: 171 us -> 265 us
  waiting for transfers between devices: 68.2 us -> 124 us
  blocking collectives: 16.4 us -> 48.5 us
  local copies, waits for them, and re-layouts: 13.2 us -> 19.1 us
    all_to_all x1, waiting for transfers between devices: 21.8 us -> 124 us  [shards(): lax.all_to_all(jnp.tile(rows, repeats), 'sp', split_axis=0, concat_axis=0...]
    all_gather x1 -> x0, waiting for transfers between devices: 45 us -> none  [shards(): piece = lax.all_gather(rows, 'sp', axis=0, tiled=True)]
    all_to_all x0 -> x1, blocking collectives: none -> 33.8 us  [copy_for_each(): lax.all_to_all(jnp.broadcast_to(shard[None], (count, *shard.shape)), axis...]
    another operation x3 -> x4, local copies, waits for them, and re-layouts: 1.78 us -> 7.11 us  [the longest x1 5.33 us: shards(): jnp.tile(rows, repeats)]
  transfers between devices with their start and end apart: 3 -> 2, of which waited for: 2 -> 1; matrix products, arithmetic and copies ran while one was open for 33% -> 21% of each run, Pallas kernels for 0% -> 0%
where the time goes in v1:
time: 270 us; the launch traced here: 265 us
  waiting for transfers between devices  124 us (46%)
  blocking collectives  48.5 us (18%)
  matrix products  38.8 us (14%)
  local copies, waits for them, and re-layouts  19.1 us (7%)
  between operations  15 us (6%)
  other arithmetic  11.8 us (4%)
  starting transfers between devices  7.26 us (3%)
    all_to_all x1, waiting for transfers between devices, shards(): lax.all_to_all(jnp.tile(rows, repeats), 'sp', split_axis=0, concat_axis=0...  124 us
    all_to_all x1, blocking collectives, copy_for_each(): lax.all_to_all(jnp.broadcast_to(shard[None], (count, *shard.shape)), axis...  33.8 us
    dot_general x8, matrix products, advance(): jnp.einsum('hij,jhv->ihv', inner.astype(jnp.bfloat16), value_block, prefe...  17.3 us
    all_to_all x1, blocking collectives, shards(): lax.all_to_all(normed, 'sp', split_axis=0, concat_axis=1, tiled=True)  14.7 us
    dot_general x8, matrix products, advance(): jnp.einsum('jhd,jhv->hdv', key_wide, value_block.astype(jnp.float32))  8.42 us
    all_to_all x1, starting transfers between devices, shards(): lax.all_to_all(jnp.tile(rows, repeats), 'sp', split_axis=0, concat_axis=0...  7.22 us
    dot_general x1, matrix products, shards(): jnp.dot(piece, own_whole, preferred_element_type=jnp.float32)  5.77 us
    dot_general x1, matrix products, shards(): jnp.dot(by_token, lax.all_gather(output_weight, 'dp', axis=0, tiled=True)...  5.46 us
  transfers between devices with their start and end apart: 2, of which 1 were waited for; matrix products, arithmetic and copies ran while one was open for 21% of the time, Pallas kernels for 0%

profile of v1, /device:TPU:32, one launch (start us, length us, event | category | flops | bytes accessed | tf_op | source)
XLA Modules:
  0.0 265.3 jit_solution(2221008132712319299)
XLA Ops:
  6.5 1.0 copy-done
  7.6 0.9 constant_dynamic-slice_fusion.1
  8.7 33.8 %all_to_all.29 = bf16[16,128,256]{2,1,0:T(8,128)(2,1)S(1)} all-to-all(bf16[16,128,256]{2,1,0:T(8,128)(2,1)S(1)} %broadcast_in_dim.18), channel_id=1, replica_groups=mesh['sp'=16,'dp'=16] {'dp'}, dimensions={0} | all-to-all | bytes 2097152 | tf_op jit(solution)/shard_map/all_to_all | solution.py:20
  42.5 5.3 %tile.9 = bf16[16,128,2048]{2,1,0:T(8,128)(2,1)} broadcast(bf16[128,2048]{1,0:T(8,128)(2,1)} %bitcast.254), dimensions={1,2} | broadcast | bytes 8912896 | tf_op jit(solution)/shard_map/tile | solution.py:121
  47.8 7.2 %all-to-all-start.1 = ((bf16[16,128,2048]{2,1,0:T(8,128)(2,1)}), bf16[16,128,2048]{2,1,0:T(8,128)(2,1)}, u32[]{:S(2)}, u32[]{:S(2)}) async-start(bf16[16,128,2048]{2,1,0:T(8,128)(2,1)} %tile.9), calls=%async_computation.1 | async-start | bytes 16777216 | tf_op jit(solution)/shard_map/all_to_all | solution.py:121
  55.1 0.7 all-gather.2.cloned.1.call-update
  55.8 0.6 fusion.109
  57.8 123.8 %all-to-all-done.1 = bf16[16,128,2048]{2,1,0:T(8,128)(2,1)} async-done(((bf16[16,128,2048]{2,1,0:T(8,128)(2,1)}), bf16[16,128,2048]{2,1,0:T(8,128)(2,1)}, u32[]{:S(2)}, u32[]{:S(2)}) %all-to-all-start.1) | async-done | bytes 8388640 | tf_op jit(solution)/shard_map/all_to_all | solution.py:121
  181.6 5.8 %fusion.104 = bf16[2048,256]{0,1:T(8,128)(2,1)S(1)} fusion(bf16[2048,256]{1,0:T(8,128)(2,1)S(1)} %bitcast.251, bf16[2048,2048]{1,0:T(8,128)(2,1)} %bitcast.3), kind=kOutput, calls=%fused_computation.101 | convolution fusion | flops 2148007936 | bytes 10485760 | tf_op jit(solution)/shard_map/dot_general | solution.py:123
  187.4 1.0 copy.52
  188.4 1.6 reverse.3
  190.2 1.2 subtract_convert_fusion
  191.5 0.7 copy.78
  192.2 0.7 copy.80
  192.9 1.4 rev.14
  194.3 1.4 rev.13
  195.7 0.8 copy.76
  196.8 16.8 %while.31 = (s32[]{:T(128)}, f32[1,64,128]{2,1,0:T(8,128)S(1)}, f32[4,512,1,128]{3,1,0,2:T(8,128)S(1)}, f32[1,1,1]{2,1,0:T(1,128)}, bf16[4,512,1,64]{1,3,2,0:T(8...) while((s32[]{:T(128)}, f32[1,64,128]{2,1,0:T(8,128)S(1)}, ...), condition=%wide.region_3.4_spmd.clone.clone.clone, body=%wide.region_2.3_spmd.clone.clone.clone.sunk | while | flops 119506944 | bytes 2469500 | solution.py:81
  196.8 2.1 fusion.152
  199.0 0.6 multiply_exponential_fusion.7
  200.0 1.0 fusion.151
  201.0 2.1 fusion.152
  203.2 0.6 multiply_exponential_fusion.7
  204.2 1.0 fusion.151
  205.2 2.1 fusion.152
  207.4 0.6 multiply_exponential_fusion.7
  208.4 1.0 fusion.151
  209.4 2.1 fusion.152
  211.6 0.6 multiply_exponential_fusion.7
  212.6 1.0 fusion.151
  214.0 0.9 pad_maximum_fusion.1
  214.9 1.7 pad_maximum_fusion
  216.7 17.5 %while.30 = (s32[]{:T(128)}, f32[1,64,128]{2,1,0:T(8,128)S(1)}, f32[4,512,1,128]{3,1,0,2:T(8,128)S(1)}, f32[1,1,1]{2,1,0:T(1,128)}, bf16[4,512,1,64]{1,3,2,0:T(8...) while((s32[]{:T(128)}, f32[1,64,128]{2,1,0:T(8,128)S(1)}, ...), condition=%wide.region_1.2_spmd.clone.clone.clone, body=%wide.region_0.1_spmd.clone.clone.clone.sunk | while | flops 119506944 | bytes 2469500 | solution.py:81
  216.7 2.2 fusion.142
  218.9 0.6 multiply_exponential_fusion.6
  219.9 1.1 fusion.141
  221.0 2.2 fusion.142
  223.2 0.6 multiply_exponential_fusion.6
  224.3 1.1 fusion.141
  225.4 2.2 fusion.142
  227.6 0.6 multiply_exponential_fusion.6
  228.6 1.1 fusion.141
  229.8 2.2 fusion.142
  232.0 0.6 multiply_exponential_fusion.6
  233.0 1.1 fusion.141
  236.3 1.0 reduce.2
  237.4 14.7 %all_to_all.30 = bf16[16,2,8192]{2,1,0:T(2,128)(2,1)S(1)} all-to-all(bf16[16,2,8192]{2,1,0:T(2,128)(2,1)S(1)} %reshape.748), channel_id=1, replica_groups=mesh['sp'=16,'dp'=16] {'sp'}, dimensions={0} | all-to-all | bytes 1048576 | tf_op jit(solution)/shard_map/all_to_all | solution.py:129
  253.0 5.5 %fusion.105 = bf16[1,128,2048]{2,1,0:T(8,128)(2,1)} fusion(bf16[128,2048]{0,1:T(8,128)(2,1)S(1)} %bitcast.242, bf16[2048,2048]{1,0:T(8,128)(2,1)} %all-gather.2.cloned.1.call-done), kind=kOutput, calls=%fused_computation.103 | convolution fusion | flops 1074003968 | bytes 9437184 | tf_op jit(solution)/shard_map/dot_general | solution.py:132
  (57 shorter events, 7.4 us)
Async XLA Ops:
  6.5 1.0 copy-start
  47.8 8.0 %copy-start.1 = (f32[2,1]{0,1:T(1,128)S(1)}, f32[2,1]{0,1:T(1,128)}, u32[]{:S(2)}) copy-start(f32[2,1]{0,1:T(1,128)} %param.15) | copy-start | bytes 28
  47.8 133.7 %all-to-all-start.1 = ((bf16[16,128,2048]{2,1,0:T(8,128)(2,1)}), bf16[16,128,2048]{2,1,0:T(8,128)(2,1)}, u32[]{:S(2)}, u32[]{:S(2)}) async-start(bf16[16,128,2048]{2,1,0:T(8,128)(2,1)} %tile.9), calls=%async_computation.1 | async-start | bytes 16777216 | tf_op jit(solution)/shard_map/all_to_all | solution.py:121
  55.1 197.9 %all-gather.2.cloned.1.call-start = ((), (), s32[]{:S(2)}) async-start(), calls=%async_computation.3 | async-start | bytes 8912896 | tf_op jit(solution)/shard_map/all_gather | solution.py:134
Sparse Core Ops, SparseCore 0:
  57.7 54.1 all-gather.1
